TPU v7x, 32 devices: a whole 2x2x4 slice. The times are simulated.
32 devices in a mesh: grp: 2 (over y), dp: 2 (over x), kv: 4 (over z), tp: 2 (over core).
Axes of the slice: x: 2, y: 2, z: 4, core: 2. Of those that a mesh axis runs over, the one named last changes fastest.
Arguments:
- queries: bfloat16 [4, 1024, 2048], P(('grp', 'dp'), 'kv', 'tp'), parts along dimension 0, may hold values from -10 to 10
- keys: bfloat16 [4, 1024, 512], P(('grp', 'dp'), 'kv', 'tp'), parts along dimension 0, may hold values from -10 to 10
- values: bfloat16 [4, 1024, 512], P(('grp', 'dp'), 'kv', 'tp'), parts along dimension 0, may hold values from -6 to 6
- gate_logits: float32 [4, 2, 1024, 32], P(('grp', 'dp'), None, 'kv', 'tp'), parts along dimension 0, may hold values from -6 to 6
- chosen: int32 [4, 8, 8, 16], P(('grp', 'dp'), 'kv', 'tp'), parts along dimension 0, may hold values from -1 to 15, as said below
- pool_k: float32 [32, 64], replicated, may hold values from 0 to 0.35
- pool_v: float32 [32, 64], replicated, may hold values from 0 to 0.35
- out_gain: float32 [2048], P('tp'), may hold values from 0.1 to 1.9
Outputs:
- attended: bfloat16 [4, 1024, 2048], P(('grp', 'dp'), 'kv', 'tp'), parts along dimension 0
There are 2 independent parts, one for each index of `grp`. A program takes and returns all parts, laid end to end along the dimension named above; an argument that names none is the same for every part. Nothing has to cross between parts.
Inputs may be any that keep to these rules, and one draw needn't show every extreme that they name: Entries are key block numbers (block e holds positions e * 64 to e * 64 + 63) or -1 for none. The list of query block b (positions b * 128 onward) holds the blocks that contain its own positions, other distinct blocks that begin before it, and -1 in its remaining entries. For the query blocks of one span of 256 positions and one key head, the blocks chosen from any other span number at most 2; in every draw some span reaches 2.
All inputs are finite; a program needn't handle non-finite values.
Results may differ from a plain program's by a relative error of at most 0.0079.
Values may be sent and summed in bfloat16 or wider, within the bound.
A program may use at most 64 MiB of HBM per device.

v0:
```python
import jax
import jax.numpy as jnp
from jax import lax
from jax.sharding import PartitionSpec as P

DH = 64
CMP_STRIDE = 16
CMP_BLOCK = 32
SLC = 64
QB = 128
NSEL = 16
MOST = 2
THETA = 500000.0
EPS = 1e-06
NEG = -1e30


def shifted(block, axis, distance):
    devices = range(lax.axis_size(axis))
    route = [(i - distance, i) for i in devices if i - distance in devices]
    return lax.ppermute(block, axis, route)


def rotate(matrix, start, heads):
    length = matrix.shape[0]
    half = DH // 2
    place = (start + jnp.arange(length)).astype(jnp.float32)
    freq = jnp.power(jnp.float32(THETA), -(2.0 * jnp.arange(half).astype(jnp.float32)) / DH)
    angle = place[:, None] * freq[None, :]
    cosine = jnp.cos(angle)[:, None, :]
    sine = jnp.sin(angle)[:, None, :]
    parts = matrix.reshape(length, heads, DH).astype(jnp.float32)
    first = parts[..., :half]
    second = parts[..., half:]
    turned = jnp.concatenate([first * cosine - second * sine, second * cosine + first * sine], -1)
    return turned.reshape(length, heads * DH).astype(jnp.bfloat16)


def compress(extended, pool, groups):
    count = extended.shape[0] // CMP_STRIDE - 1
    parts = extended.reshape(count + 1, CMP_STRIDE, groups, DH).astype(jnp.float32)
    lower = jnp.einsum(
        "nigd,id->ngd", parts[:-1], pool[:CMP_STRIDE], precision=lax.Precision.HIGHEST
    )
    upper = jnp.einsum(
        "nigd,id->ngd", parts[1:], pool[CMP_STRIDE:], precision=lax.Precision.HIGHEST
    )
    return (lower + upper).astype(jnp.bfloat16)


def wanted_blocks(lists, owners, per_owner):
    groups = lists.shape[1]
    total = owners * per_owner
    hits = lists[..., None] == jnp.arange(total, dtype=jnp.int32)
    member = jnp.any(hits, axis=(0, 2)).astype(jnp.int32).reshape(groups, owners, per_owner)
    rank = jnp.cumsum(member, -1) - member
    slot_hit = (member[..., None] == 1) & (rank[..., None] == jnp.arange(MOST))
    local_ids = jnp.arange(per_owner, dtype=jnp.int32)[:, None]
    asked = jnp.sum(jnp.where(slot_hit, local_ids, 0), axis=2)
    return (asked.transpose(1, 0, 2), rank.reshape(groups, total))


def per_device(queries, keys, values, gate_logits, chosen, pool_k, pool_v, out_gain):
    queries = queries[0]
    keys = keys[0]
    values = values[0]
    logits = gate_logits[0]
    lists = chosen[0]
    length = queries.shape[0]
    groups = keys.shape[1] // DH
    heads = queries.shape[1] // DH
    per_group = heads // groups
    qblocks = length // QB
    owners = lax.axis_size("kv")
    myself = lax.axis_index("kv")
    start = myself * length
    scale = DH ** (-0.5)
    query_turned = rotate(queries, start, heads)
    key_turned = rotate(keys, start, groups)
    next_keys, next_values = shifted((keys[:CMP_STRIDE], values[:CMP_STRIDE]), "kv", -1)
    key_summary = compress(jnp.concatenate([keys, next_keys], 0), pool_k, groups)
    value_summary = compress(jnp.concatenate([values, next_values], 0), pool_v, groups)
    place = start + jnp.arange(length)
    query_group = queries.reshape(length, groups, per_group, DH).transpose(1, 2, 0, 3)
    part_keys = lax.all_gather(key_summary, "kv", axis=0, tiled=True)
    part_values = lax.all_gather(value_summary, "kv", axis=0, tiled=True)
    count = part_keys.shape[0]
    ends = jnp.arange(count) * CMP_STRIDE + CMP_BLOCK - 1
    allow = ends[None, :] <= place[:, None]

    def per_group_fold(item):
        query_part, key_part, value_part, top, total, summed = item
        score = (
            jnp.einsum("htd,nd->htn", query_part, key_part, preferred_element_type=jnp.float32)
            * scale
        )
        score = jnp.where(allow, score, NEG)
        fresh = jnp.maximum(top, jnp.max(score, -1))
        weight = jnp.where(allow, jnp.exp(score - fresh[..., None]), 0.0)
        shrink = jnp.exp(top - fresh)
        total = total * shrink + jnp.sum(weight, -1)
        summed = summed * shrink[..., None] + jnp.einsum(
            "htn,nd->htd",
            weight.astype(jnp.bfloat16),
            value_part,
            preferred_element_type=jnp.float32,
        )
        return (fresh, total, summed)

    top = jnp.full((groups, per_group, length), NEG, jnp.float32)
    total = jnp.zeros((groups, per_group, length), jnp.float32)
    summed = jnp.zeros((groups, per_group, length, DH), jnp.float32)
    top, total, summed = lax.map(
        per_group_fold,
        (
            query_group,
            part_keys.transpose(1, 0, 2),
            part_values.transpose(1, 0, 2),
            top,
            total,
            summed,
        ),
    )
    summary_out = summed / jnp.maximum(total, 1.0)[..., None]
    group_pick = jnp.arange(groups)[None, :, None]
    safe = jnp.maximum(lists, 0)
    per_owner = length // SLC
    asked_ids, rank = wanted_blocks(lists, owners, per_owner)
    requests = lax.all_to_all(asked_ids, "kv", split_axis=0, concat_axis=0, tiled=True)
    local_keys = key_turned.reshape(per_owner, SLC, groups, DH)
    local_values = values.reshape(per_owner, SLC, groups, DH)
    served = (local_keys[requests, :, group_pick, :], local_values[requests, :, group_pick, :])
    got_keys, got_values = (
        lax.all_to_all(served[0], "kv", split_axis=0, concat_axis=0, tiled=True),
        lax.all_to_all(served[1], "kv", split_axis=0, concat_axis=0, tiled=True),
    )

    def table(received, local):
        remote = received.transpose(1, 0, 2, 3, 4).reshape(groups, owners * MOST, SLC, DH)
        return jnp.concatenate([remote, local.transpose(2, 0, 1, 3)], 1)

    owner = safe // per_owner
    inner = safe % per_owner
    slot = jnp.where(owner == myself, owners * MOST + inner, owner * MOST + rank[group_pick, safe])
    key_sel = table(got_keys, local_keys)[group_pick, slot]
    value_sel = table(got_values, local_values)[group_pick, slot]
    query_blocks = query_turned.reshape(qblocks, QB, groups, per_group, DH)

    def attend(item):
        index, query_part, keys_part, values_part, picks = item
        place_q = start + index * QB + jnp.arange(QB)
        score = jnp.einsum(
            "tghd,gnkd->ghtnk", query_part, keys_part, preferred_element_type=jnp.float32
        )
        score = score.reshape(groups, per_group, QB, NSEL * SLC) * scale
        safe_picks = jnp.maximum(picks, 0)
        key_place = (safe_picks[..., None] * SLC + jnp.arange(SLC)).reshape(groups, NSEL * SLC)
        live = jnp.broadcast_to(picks[..., None] >= 0, (groups, NSEL, SLC)).reshape(
            groups, NSEL * SLC
        )
        allow = (live[:, None, :] & (key_place[:, None, :] <= place_q[None, :, None]))[:, None]
        score = jnp.where(allow, score, NEG)
        top_sel = jnp.max(score, -1, keepdims=True)
        weight = jnp.where(allow, jnp.exp(score - top_sel), 0.0)
        total_sel = jnp.sum(weight, -1)
        flat_values = values_part.reshape(groups, NSEL * SLC, DH)
        out = jnp.einsum(
            "ghtk,gkd->ghtd",
            weight.astype(jnp.bfloat16),
            flat_values,
            preferred_element_type=jnp.float32,
        )
        return out / total_sel[..., None]

    chosen_out = lax.map(attend, (jnp.arange(qblocks), query_blocks, key_sel, value_sel, lists))
    gates = jax.nn.sigmoid(logits)
    summary_rows = summary_out.transpose(2, 0, 1, 3).reshape(length, heads, DH)
    chosen_rows = chosen_out.transpose(0, 3, 1, 2, 4).reshape(length, heads, DH)
    mixed = gates[0][..., None] * summary_rows + gates[1][..., None] * chosen_rows
    normed = (
        mixed
        * lax.rsqrt(jnp.mean(mixed * mixed, -1, keepdims=True) + EPS)
        * out_gain.reshape(heads, DH)
    )
    return normed.reshape(1, length, heads * DH).astype(jnp.bfloat16)


def solution(mesh):
    in_specs = (
        P(("grp", "dp"), "kv", "tp"),
        P(("grp", "dp"), "kv", "tp"),
        P(("grp", "dp"), "kv", "tp"),
        P(("grp", "dp"), None, "kv", "tp"),
        P(("grp", "dp"), "kv", "tp", None),
        P(),
        P(),
        P("tp"),
    )
    out_specs = P(("grp", "dp"), "kv", "tp")
    return jax.shard_map(
        per_device, mesh=mesh, in_specs=in_specs, out_specs=out_specs, check_vma=False
    )
```

profile of v0, /device:TPU:0, one launch (start us, length us, event | category | flops | bytes accessed | tf_op | source)
XLA Modules:
  0.0 114.5 jit_solution(15482757723917872336)
XLA Ops:
  2.6 6.3 %all-to-all-start = ((s32[4,4,2]{1,2,0:T(2,128)}), s32[4,4,2]{1,2,0:T(2,128)S(1)}, u32[]{:S(2)}, u32[]{:S(2)}) async-start(s32[4,4,2]{1,2,0:T(2,128)} %copy.74), calls=%async_computation | async-start | bytes 8192 | tf_op jit(solution)/shard_map/all_to_all | solution.py:129
  9.6 1.3 %collective-permute-start.1 = (bf16[16,256]{1,0:T(8,128)(2,1)S(1)}, bf16[16,256]{1,0:T(8,128)(2,1)S(1)}, u32[]{:S(2)}, u32[]{:S(2)}) collective-permute-start(bf16[16,256]{1,0:T(8,128)(2,1)S(1)} %slice_bitcast_fusion.1), channel_id=1, source_target_pairs={{2,0},{4,2},{6,4},{3,1},{5,3},{7,5},{10,8},{12,10},{14,12},{11,9},... | collective-permute-start | bytes 24584 | tf_op jit(solution)/shard_map/ppermute | solution.py:21
  11.6 1.3 %collective-permute-start = (bf16[16,256]{1,0:T(8,128)(2,1)S(1)}, bf16[16,256]{1,0:T(8,128)(2,1)S(1)}, u32[]{:S(2)}, u32[]{:S(2)}) collective-permute-start(bf16[16,256]{1,0:T(8,128)(2,1)S(1)} %slice_bitcast_fusion.4), channel_id=1, source_target_pairs={{2,0},{4,2},{6,4},{3,1},{5,3},{7,5},{10,8},{12,10},{14,12},{11,9},... | collective-permute-start | bytes 24584 | tf_op jit(solution)/shard_map/ppermute | solution.py:21
  18.1 1.5 %gather_fusion.1 = s32[128]{0:T(128)S(1)} fusion(s32[4,16]{1,0:T(4,128)S(1)} %convert_subtract_fusion, s32[128]{0:T(128)S(1)} %reshape.454), kind=kCustom, calls=%fused_computation.1 | custom fusion | bytes 2048 | tf_op jit(solution)/shard_map/gather | solution.py:144
  26.7 1.1 reshape.513
  27.8 7.4 %all-to-all-start.2 = ((bf16[4,2,16384]{2,1,0:T(2,128)(2,1)}), bf16[4,2,16384]{2,1,0:T(2,128)(2,1)S(1)}, u32[]{:S(2)}, u32[]{:S(2)}) async-start(bf16[4,2,16384]{2,1,0:T(2,128)(2,1)} %reshape.513), calls=%async_computation.2 | async-start | bytes 524288 | tf_op jit(solution)/shard_map/all_to_all | solution.py:135
  35.9 1.1 reshape.511
  37.6 13.7 %all_gather.7 = bf16[64,4,64]{2,1,0:T(4,128)(2,1)S(1)} all-gather(bf16[16,4,64]{2,1,0:T(4,128)(2,1)S(1)} %fusion.39), channel_id=1, replica_groups=mesh['grp'=2,'dp'=2,'kv'=4,'tp'=2] {'kv'}, dimensions={0}, use_global_device_ids=true | all-gather | bytes 40960 | tf_op jit(solution)/shard_map/all_gather | solution.py:86
  51.6 13.3 %all_gather.6 = bf16[64,4,64]{2,0,1:T(8,128)(2,1)S(1)} all-gather(bf16[16,4,64]{2,0,1:T(8,128)(2,1)S(1)} %fusion.40), channel_id=1, replica_groups=mesh['grp'=2,'dp'=2,'kv'=4,'tp'=2] {'kv'}, dimensions={0}, use_global_device_ids=true | all-gather | bytes 40960 | tf_op jit(solution)/shard_map/all_gather | solution.py:85
  64.9 4.6 %all-to-all-start.1 = ((bf16[4,2,16384]{2,1,0:T(2,128)(2,1)}), bf16[4,2,16384]{2,1,0:T(2,128)(2,1)S(1)}, u32[]{:S(2)}, u32[]{:S(2)}) async-start(bf16[4,2,16384]{2,1,0:T(2,128)(2,1)} %reshape.511), calls=%async_computation.1 | async-start | bytes 524288 | tf_op jit(solution)/shard_map/all_to_all | solution.py:134
  69.5 5.2 %while.24 = (s32[]{:T(128)}, f32[4,4,256]{2,1,0:T(4,128)S(1)}, f32[4,4,256,64]{2,3,1,0:T(8,128)}, bf16[4,4,256,64]{2,3,1,0:T(8,128)(2,1)S(1)}, bf16[4,64,64]{2,1...) while((s32[]{:T(128)}, f32[4,4,256]{2,1,0:T(4,128)S(1)}, ...), condition=%wide.region_3.4_spmd.clone, body=%wide.region_0.3_spmd.clone.sunk | while | flops 17454080 | bytes 1326441 | solution.py:113
  75.1 1.2 %all-to-all-done.1 = bf16[4,2,16384]{2,1,0:T(2,128)(2,1)S(1)} async-done(((bf16[4,2,16384]{2,1,0:T(2,128)(2,1)}), bf16[4,2,16384]{2,1,0:T(2,128)(2,1)S(1)}, u32[]{:S(2)}, u32[]{:S(2)}) %all-to-all-start.1) | async-done | bytes 262176 | tf_op jit(solution)/shard_map/all_to_all | solution.py:134
  77.0 2.3 %gather_fusion.2 = bf16[128,64,64]{2,1,0:T(8,128)(2,1)} fusion(bf16[4,12,64,64]{3,2,1,0:T(8,128)(2,1)S(1)} %pad_maximum_fusion, s32[128]{0:T(128)S(1)} %reshape.460), kind=kCustom, calls=%fused_computation.2 | custom fusion | bytes 2098176 | tf_op jit(solution)/shard_map/gather | solution.py:145
  80.5 28.3 %while.23 = (s32[]{:T(128)}, f32[2,4,4,128,64]{3,4,2,1,0:T(8,128)}, s32[2,4,16]{2,1,0:T(4,128)S(1)}, s32[2]{0:T(128)S(1)}, s32[]{:T(128)}, /*index=5*/bf16[2,4,1...) while((s32[]{:T(128)}, f32[2,4,4,128,64]{3,4,2,1,0:T(8,128)}, ...), condition=%wide.region_10.11_spmd, body=%wide.region_7.10_spmd.sunk | while | flops 562172224 | bytes 65482908 | solution.py:175
  83.3 1.4 %compare_and_fusion.5 = pred[4,128,1024]{1,2,0:T(8,128)(4,1)S(1)} fusion(s32[128]{0:T(128)S(1)} %iota_add_fusion.5, s32[4,1024]{1,0:T(4,128)S(1)} %broadcast_add_fusion.2, pred[4,1024]{1,0:T(4,128)(4,1)S(1)} %and.110), kind=kLoop, calls=%fused_computation.15.clone.1 | loop fusion | flops 1048576 | bytes 545280 | tf_op jit(solution)/shard_map/while/body/eval_jaxpr/and | solution.py:161
  84.8 2.5 %select_reduce_fusion.5 = (f32[4,4,128]{2,1,0:T(4,128)S(1)}, f32[4,4,128,16,64]{2,4,1,3,0:T(8,128)S(1)}) fusion(pred[4,128,16,64]{1,3,2,0:T(8,128)(4,1)S(1)} %compare_and_fusion.4, bf16[2,128,4,4,64]{1,4,3,2,0:T(8,128)(2,1)} %get-tuple-element.346, s32[]{:T(128)S(6)} %copy.143, bf16[2,4,16,64,64]{4,3,2,1,0:T(8,128)(2,1)} %get-tuple-element.345), kind=kOutput, calls=%fused_computation.13.clone.1 | convolution fusion | flops 274724864 | bytes 10232832 | tf_op jit(solution)/shard_map/while/body/eval_jaxpr/tghd,gnkd->ghtnk/dot_general | solution.py:152
  87.3 2.1 %select_reduce_fusion.6 = f32[4,4,128]{2,1,0:T(4,128)S(1)} fusion(f32[4,4,128,16,64]{2,4,1,3,0:T(8,128)S(1)} %get-tuple-element.306, f32[4,4,128]{2,1,0:T(4,128)S(1)} %get-tuple-element.307, pred[4,128,16,64]{1,3,2,0:T(8,128)(4,1)S(1)} %compare_and_fusion.4), kind=kLoop, calls=%fused_computation.11.clone.1 | loop fusion | flops 8386560 | bytes 8929280 | tf_op jit(solution)/shard_map/while/body/eval_jaxpr/reduce_sum | solution.py:165
  90.3 2.4 %fusion.68 = bf16[4,4,128,1024]{2,3,1,0:T(8,128)(2,1)S(1)} fusion(f32[4,4,128,16,64]{2,4,3,1,0:T(8,128)S(1)} %copy.137, f32[4,4,128]{2,1,0:T(4,128)S(1)} %get-tuple-element.307, pred[4,128,1024]{1,2,0:T(8,128)(4,1)S(1)} %compare_and_fusion.5), kind=kLoop, calls=%fused_computation.10.clone.1 | loop fusion | flops 8388608 | bytes 13115392 | tf_op jit(solution)/shard_map/while/body/eval_jaxpr/convert_element_type | solution.py:169
  97.4 1.4 %compare_and_fusion.5 = pred[4,128,1024]{1,2,0:T(8,128)(4,1)S(1)} fusion(s32[128]{0:T(128)S(1)} %iota_add_fusion.5, s32[4,1024]{1,0:T(4,128)S(1)} %broadcast_add_fusion.2, pred[4,1024]{1,0:T(4,128)(4,1)S(1)} %and.110), kind=kLoop, calls=%fused_computation.15.clone.1 | loop fusion | flops 1048576 | bytes 545280 | tf_op jit(solution)/shard_map/while/body/eval_jaxpr/and | solution.py:161
  98.9 2.5 %select_reduce_fusion.5 = (f32[4,4,128]{2,1,0:T(4,128)S(1)}, f32[4,4,128,16,64]{2,4,1,3,0:T(8,128)S(1)}) fusion(pred[4,128,16,64]{1,3,2,0:T(8,128)(4,1)S(1)} %compare_and_fusion.4, bf16[2,128,4,4,64]{1,4,3,2,0:T(8,128)(2,1)} %get-tuple-element.346, s32[]{:T(128)S(6)} %copy.143, bf16[2,4,16,64,64]{4,3,2,1,0:T(8,128)(2,1)} %get-tuple-element.345), kind=kOutput, calls=%fused_computation.13.clone.1 | convolution fusion | flops 274724864 | bytes 10232832 | tf_op jit(solution)/shard_map/while/body/eval_jaxpr/tghd,gnkd->ghtnk/dot_general | solution.py:152
  101.4 2.1 %select_reduce_fusion.6 = f32[4,4,128]{2,1,0:T(4,128)S(1)} fusion(f32[4,4,128,16,64]{2,4,1,3,0:T(8,128)S(1)} %get-tuple-element.306, f32[4,4,128]{2,1,0:T(4,128)S(1)} %get-tuple-element.307, pred[4,128,16,64]{1,3,2,0:T(8,128)(4,1)S(1)} %compare_and_fusion.4), kind=kLoop, calls=%fused_computation.11.clone.1 | loop fusion | flops 8386560 | bytes 8929280 | tf_op jit(solution)/shard_map/while/body/eval_jaxpr/reduce_sum | solution.py:165
  104.4 2.4 %fusion.68 = bf16[4,4,128,1024]{2,3,1,0:T(8,128)(2,1)S(1)} fusion(f32[4,4,128,16,64]{2,4,3,1,0:T(8,128)S(1)} %copy.137, f32[4,4,128]{2,1,0:T(4,128)S(1)} %get-tuple-element.307, pred[4,128,1024]{1,2,0:T(8,128)(4,1)S(1)} %compare_and_fusion.5), kind=kLoop, calls=%fused_computation.10.clone.1 | loop fusion | flops 8388608 | bytes 13115392 | tf_op jit(solution)/shard_map/while/body/eval_jaxpr/convert_element_type | solution.py:169
  108.7 1.6 %fusion.33 = (f32[256,4,4]{0,2,1:T(4,128)S(1)}, f32[4,4,256,64]{2,3,1,0:T(8,128)S(1)}) fusion(f32[256,4,4]{0,2,1:T(4,128)S(1)} %mul.290, f32[256,4,4]{0,2,1:T(4,128)S(1)} %mul.287, f32[4,4,256,64]{2,3,1,0:T(8,128)S(1)} %copy-done.4, f32[4,4,256]{2,1,0:T(4,128)S(1)} %broadcast_maximum_fusion.1, f32[2,4,4,128,64]{3,4,2,1,0:T(8,128)} %get-tuple-element.87), kind=kLoop, calls=%fused_computation.57 | loop fusion | flops 1568768 | bytes 3211264 | tf_op jit(solution)/shard_map/reduce_sum | solution.py:182
  110.3 2.0 %copy.86 = f32[2,128,4,4,64]{1,0,4,3,2:T(2,128)S(1)} copy(f32[2,128,4,4,64]{1,4,3,2,0:T(8,128)} %bitcast.233) | data formatting | bytes 2097152 | tf_op jit(solution)/shard_map/transpose | solution.py:178
  (160 shorter events, 36.7 us)
Async XLA Ops:
  0.0 23.6 %copy-start.5 = (bf16[1,256,1024]{2,1,0:T(8,128)(2,1)S(1)}, bf16[1,256,1024]{2,1,0:T(8,128)(2,1)}, u32[]{:S(2)}) copy-start(bf16[1,256,1024]{2,1,0:T(8,128)(2,1)} %param.12) | copy-start | bytes 1572868
  2.6 23.2 %all-to-all-start = ((s32[4,4,2]{1,2,0:T(2,128)}), s32[4,4,2]{1,2,0:T(2,128)S(1)}, u32[]{:S(2)}, u32[]{:S(2)}) async-start(s32[4,4,2]{1,2,0:T(2,128)} %copy.74), calls=%async_computation | async-start | bytes 8192 | tf_op jit(solution)/shard_map/all_to_all | solution.py:129
  9.6 27.4 %collective-permute-start.1 = (bf16[16,256]{1,0:T(8,128)(2,1)S(1)}, bf16[16,256]{1,0:T(8,128)(2,1)S(1)}, u32[]{:S(2)}, u32[]{:S(2)}) collective-permute-start(bf16[16,256]{1,0:T(8,128)(2,1)S(1)} %slice_bitcast_fusion.1), channel_id=1, source_target_pairs={{2,0},{4,2},{6,4},{3,1},{5,3},{7,5},{10,8},{12,10},{14,12},{11,9},... | collective-permute-start | bytes 24584 | tf_op jit(solution)/shard_map/ppermute | solution.py:21
  11.6 25.8 %collective-permute-start = (bf16[16,256]{1,0:T(8,128)(2,1)S(1)}, bf16[16,256]{1,0:T(8,128)(2,1)S(1)}, u32[]{:S(2)}, u32[]{:S(2)}) collective-permute-start(bf16[16,256]{1,0:T(8,128)(2,1)S(1)} %slice_bitcast_fusion.4), channel_id=1, source_target_pairs={{2,0},{4,2},{6,4},{3,1},{5,3},{7,5},{10,8},{12,10},{14,12},{11,9},... | collective-permute-start | bytes 24584 | tf_op jit(solution)/shard_map/ppermute | solution.py:21
  19.6 17.4 %copy-start.2 = (bf16[1,256,256]{2,1,0:T(8,128)(2,1)S(1)}, bf16[1,256,256]{2,1,0:T(8,128)(2,1)}, u32[]{:S(2)}) copy-start(bf16[1,256,256]{2,1,0:T(8,128)(2,1)} %param.14) | copy-start | bytes 393220
  22.8 14.6 %copy-start.3 = (bf16[1,256,256]{2,1,0:T(8,128)(2,1)S(1)}, bf16[1,256,256]{2,1,0:T(8,128)(2,1)}, u32[]{:S(2)}) copy-start(bf16[1,256,256]{2,1,0:T(8,128)(2,1)} %param.13) | copy-start | bytes 393220
  27.8 37.1 %all-to-all-start.2 = ((bf16[4,2,16384]{2,1,0:T(2,128)(2,1)}), bf16[4,2,16384]{2,1,0:T(2,128)(2,1)S(1)}, u32[]{:S(2)}, u32[]{:S(2)}) async-start(bf16[4,2,16384]{2,1,0:T(2,128)(2,1)} %reshape.513), calls=%async_computation.2 | async-start | bytes 524288 | tf_op jit(solution)/shard_map/all_to_all | solution.py:135
  64.9 11.4 %all-to-all-start.1 = ((bf16[4,2,16384]{2,1,0:T(2,128)(2,1)}), bf16[4,2,16384]{2,1,0:T(2,128)(2,1)S(1)}, u32[]{:S(2)}, u32[]{:S(2)}) async-start(bf16[4,2,16384]{2,1,0:T(2,128)(2,1)} %reshape.511), calls=%async_computation.1 | async-start | bytes 524288 | tf_op jit(solution)/shard_map/all_to_all | solution.py:134
  74.7 5.7 %copy-start.6 = (s32[1,2,4,16]{3,2,1,0:T(4,128)S(1)}, s32[1,2,4,16]{3,2,1,0:T(4,128)}, u32[]{:S(2)}) copy-start(s32[1,2,4,16]{3,2,1,0:T(4,128)} %param.16) | copy-start | bytes 1540
  80.4 28.3 %copy-start.4 = (f32[4,4,256,64]{2,3,1,0:T(8,128)S(1)}, f32[4,4,256,64]{2,3,1,0:T(8,128)}, u32[]{:S(2)}) copy-start(f32[4,4,256,64]{2,3,1,0:T(8,128)} %get-tuple-element.85) | copy-start | bytes 3145732
  80.4 32.8 %copy-start.7 = (f32[1024]{0:T(1024)S(1)}, f32[1024]{0:T(1024)}, u32[]{:S(2)}) copy-start(f32[1024]{0:T(1024)} %param.19) | copy-start | bytes 12292
  90.3 2.4 %copy-start = (f32[2,4,4,128,64]{3,4,2,1,0:T(8,128)S(1)}, f32[2,4,4,128,64]{3,4,2,1,0:T(8,128)}, u32[]{:S(2)}) copy-start(f32[2,4,4,128,64]{3,4,2,1,0:T(8,128)} %get-tuple-element.331) | copy-start | bytes 3145732 | tf_op jit(solution)/shard_map/while
  93.6 1.0 copy-start.1
  104.4 2.4 %copy-start = (f32[2,4,4,128,64]{3,4,2,1,0:T(8,128)S(1)}, f32[2,4,4,128,64]{3,4,2,1,0:T(8,128)}, u32[]{:S(2)}) copy-start(f32[2,4,4,128,64]{3,4,2,1,0:T(8,128)} %get-tuple-element.331) | copy-start | bytes 3145732 | tf_op jit(solution)/shard_map/while
  107.7 1.0 copy-start.1
where the time goes:
time: 115 us; the launch traced here: 114 us
  local copies, waits for them, and re-layouts  29.9 us (26%)
  blocking collectives  27 us (23%)
  other arithmetic  22.1 us (19%)
  starting transfers between devices  21 us (18%)
  matrix products  11.2 us (10%)
  loops' own time  1.71 us (1%)
  waiting for transfers between devices  1.22 us (1%)
    all_gather x1, blocking collectives, per_device(): part_values = lax.all_gather(value_summary, 'kv', axis=0, tiled=True)  13.7 us
    all_gather x1, blocking collectives, per_device(): part_keys = lax.all_gather(key_summary, 'kv', axis=0, tiled=True)  13.3 us
    all_to_all x1, starting transfers between devices, per_device(): lax.all_to_all(served[1], 'kv', split_axis=0, concat_axis=0, tiled=True)  7.44 us
    all_to_all x1, starting transfers between devices, per_device(): lax.all_to_all(asked_ids, 'kv', split_axis=0, concat_axis=0, tiled=True)  6.35 us
    unnamed x21, local copies, waits for them, and re-layouts  5.66 us
    dot_general x2, matrix products, attend(): jnp.einsum('tghd,gnkd->ghtnk', query_part, keys_part, preferred_element_t...  5.03 us
    convert_element_type x2, other arithmetic, attend(): weight.astype(jnp.bfloat16)  4.81 us
    and x4, other arithmetic, attend(): live[:, None, :] & (key_place[:, None, :] <= place_q[None, :, None])  4.65 us
  transfers between devices with their start and end apart: 5, of which 1 were waited for; matrix products, arithmetic and copies ran while one was open for 21% of the time, Pallas kernels for 0%

commit v1 on v0

--- a/solution.py
+++ b/solution.py
@@ -82,7 +82,9 @@
     value_summary = compress(jnp.concatenate([values, next_values], 0), pool_v, groups)
     place = start + jnp.arange(length)
     query_group = queries.reshape(length, groups, per_group, DH).transpose(1, 2, 0, 3)
-    part_keys = lax.all_gather(key_summary, "kv", axis=0, tiled=True)
+    part_keys = jnp.concatenate(
+        lax.all_to_all(jnp.stack([key_summary] * lax.axis_size("kv")), "kv", 0, 0), axis=0
+    )
     part_values = lax.all_gather(value_summary, "kv", axis=0, tiled=True)
     count = part_keys.shape[0]
     ends = jnp.arange(count) * CMP_STRIDE + CMP_BLOCK - 1

time: 115 us -> 108 us (0.939)
  blocking collectives: 27 us -> 14.4 us
  starting transfers between devices: 21 us -> 23.5 us
  waiting for transfers between devices: 1.22 us -> 3.09 us
    all_gather x1 -> x0, blocking collectives: 13.3 us -> none  [per_device(): part_keys = lax.all_gather(key_summary, 'kv', axis=0, tiled=True)]
    all_to_all x0 -> x1, starting transfers between devices: none -> 7.44 us  [per_device(): lax.all_to_all(jnp.stack([key_summary] * lax.axis_size('kv')), 'kv', 0, 0)]
    all_to_all x1, starting transfers between devices: 7.44 us -> 3.4 us  [per_device(): lax.all_to_all(served[1], 'kv', split_axis=0, concat_axis=0, tiled=True)]
    all_to_all x0 -> x1, waiting for transfers between devices: none -> 1.87 us  [per_device(): lax.all_to_all(jnp.stack([key_summary] * lax.axis_size('kv')), 'kv', 0, 0)]
    unnamed x21 -> x24, local copies, waits for them, and re-layouts: 5.66 us -> 6.52 us
  transfers between devices with their start and end apart: 5 -> 6, of which waited for: 1 -> 2; matrix products, arithmetic and copies ran while one was open for 21% -> 23% of each run, Pallas kernels for 0% -> 0%
where the time goes in v1:
time: 108 us; the launch traced here: 107 us
  local copies, waits for them, and re-layouts  30.8 us (29%)
  starting transfers between devices  23.5 us (22%)
  other arithmetic  22.1 us (20%)
  blocking collectives  14.4 us (13%)
  matrix products  11.2 us (10%)
  waiting for transfers between devices  3.09 us (3%)
  loops' own time  1.71 us (2%)
    all_gather x1, blocking collectives, per_device(): part_values = lax.all_gather(value_summary, 'kv', axis=0, tiled=True)  14.4 us
    all_to_all x1, starting transfers between devices, per_device(): lax.all_to_all(jnp.stack([key_summary] * lax.axis_size('kv')), 'kv', 0, 0)  7.44 us
    unnamed x24, local copies, waits for them, and re-layouts  6.52 us
    all_to_all x1, starting transfers between devices, per_device(): lax.all_to_all(asked_ids, 'kv', split_axis=0, concat_axis=0, tiled=True)  6.35 us
    dot_general x2, matrix products, attend(): jnp.einsum('tghd,gnkd->ghtnk', query_part, keys_part, preferred_element_t...  5.02 us
    convert_element_type x2, other arithmetic, attend(): weight.astype(jnp.bfloat16)  4.79 us
    and x4, other arithmetic, attend(): live[:, None, :] & (key_place[:, None, :] <= place_q[None, :, None])  4.65 us
    reduce_sum x2, other arithmetic, attend(): total_sel = jnp.sum(weight, -1)  4.23 us
  transfers between devices with their start and end apart: 6, of which 2 were waited for; matrix products, arithmetic and copies ran while one was open for 23% of the time, Pallas kernels for 0%

profile of v1, /device:TPU:0, one launch (start us, length us, event | category | flops | bytes accessed | tf_op | source)
XLA Modules:
  0.0 107.3 jit_solution(8930825560568782811)
XLA Ops:
  2.6 6.3 %all-to-all-start.1 = ((s32[4,4,2]{1,2,0:T(2,128)}), s32[4,4,2]{1,2,0:T(2,128)S(1)}, u32[]{:S(2)}, u32[]{:S(2)}) async-start(s32[4,4,2]{1,2,0:T(2,128)} %copy.95), calls=%async_computation.1 | async-start | bytes 8192 | tf_op jit(solution)/shard_map/all_to_all | solution.py:131
  9.6 1.3 %collective-permute-start.1 = (bf16[16,256]{1,0:T(8,128)(2,1)S(1)}, bf16[16,256]{1,0:T(8,128)(2,1)S(1)}, u32[]{:S(2)}, u32[]{:S(2)}) collective-permute-start(bf16[16,256]{1,0:T(8,128)(2,1)S(1)} %slice_bitcast_fusion.1), channel_id=1, source_target_pairs={{2,0},{4,2},{6,4},{3,1},{5,3},{7,5},{10,8},{12,10},{14,12},{11,9},... | collective-permute-start | bytes 24584 | tf_op jit(solution)/shard_map/ppermute | solution.py:21
  11.6 1.3 %collective-permute-start = (bf16[16,256]{1,0:T(8,128)(2,1)S(1)}, bf16[16,256]{1,0:T(8,128)(2,1)S(1)}, u32[]{:S(2)}, u32[]{:S(2)}) collective-permute-start(bf16[16,256]{1,0:T(8,128)(2,1)S(1)} %slice_bitcast_fusion.4), channel_id=1, source_target_pairs={{2,0},{4,2},{6,4},{3,1},{5,3},{7,5},{10,8},{12,10},{14,12},{11,9},... | collective-permute-start | bytes 24584 | tf_op jit(solution)/shard_map/ppermute | solution.py:21
  16.9 1.1 %slice.72 = bf16[16,16,4,64]{3,2,1,0:T(4,128)(2,1)S(1)} reshape(bf16[1,256,256]{2,1,0:T(8,128)(2,1)} %param.14) | data formatting | bytes 262144 | tf_op jit(solution)/shard_map/slice | solution.py:43
  18.2 1.5 %gather_fusion.1 = s32[128]{0:T(128)S(1)} fusion(s32[4,16]{1,0:T(4,128)S(1)} %convert_subtract_fusion, s32[128]{0:T(128)S(1)} %reshape.460), kind=kCustom, calls=%fused_computation.1 | custom fusion | bytes 2048 | tf_op jit(solution)/shard_map/gather | solution.py:146
  27.0 7.4 %all-to-all-start = ((bf16[4,2,2048]{2,1,0:T(2,128)(2,1)}), bf16[4,2,2048]{2,1,0:T(2,128)(2,1)S(1)}, u32[]{:S(2)}, u32[]{:S(2)}) async-start(bf16[4,2,2048]{2,1,0:T(2,128)(2,1)} %reshape.521), calls=%async_computation | async-start | bytes 65536 | tf_op jit(solution)/shard_map/all_to_all | solution.py:86
  38.2 1.9 %all-to-all-done = bf16[4,2,2048]{2,1,0:T(2,128)(2,1)S(1)} async-done(((bf16[4,2,2048]{2,1,0:T(2,128)(2,1)}), bf16[4,2,2048]{2,1,0:T(2,128)(2,1)S(1)}, u32[]{:S(2)}, u32[]{:S(2)}) %all-to-all-start) | async-done | bytes 32800 | tf_op jit(solution)/shard_map/all_to_all | solution.py:86
  40.1 3.4 %all-to-all-start.3 = ((bf16[4,2,16384]{2,1,0:T(2,128)(2,1)}), bf16[4,2,16384]{2,1,0:T(2,128)(2,1)S(1)}, u32[]{:S(2)}, u32[]{:S(2)}) async-start(bf16[4,2,16384]{2,1,0:T(2,128)(2,1)} %reshape.519), calls=%async_computation.3 | async-start | bytes 524288 | tf_op jit(solution)/shard_map/all_to_all | solution.py:137
  43.9 14.4 %all_gather.3 = bf16[64,4,64]{2,1,0:T(4,128)(2,1)S(1)} all-gather(bf16[16,4,64]{2,1,0:T(4,128)(2,1)S(1)} %fusion.39), channel_id=1, replica_groups=mesh['grp'=2,'dp'=2,'kv'=4,'tp'=2] {'kv'}, dimensions={0}, use_global_device_ids=true | all-gather | bytes 40960 | tf_op jit(solution)/shard_map/all_gather | solution.py:88
  58.6 3.8 %all-to-all-start.2 = ((bf16[4,2,16384]{2,1,0:T(2,128)(2,1)}), bf16[4,2,16384]{2,1,0:T(2,128)(2,1)S(1)}, u32[]{:S(2)}, u32[]{:S(2)}) async-start(bf16[4,2,16384]{2,1,0:T(2,128)(2,1)} %reshape.517), calls=%async_computation.2 | async-start | bytes 524288 | tf_op jit(solution)/shard_map/all_to_all | solution.py:136
  62.4 5.2 %while.24 = (s32[]{:T(128)}, f32[4,4,256]{2,1,0:T(4,128)S(1)}, f32[4,4,256,64]{2,3,1,0:T(8,128)}, bf16[4,4,256,64]{2,3,1,0:T(8,128)(2,1)S(1)}, bf16[4,64,64]{2,1...) while((s32[]{:T(128)}, f32[4,4,256]{2,1,0:T(4,128)S(1)}, ...), condition=%wide.region_3.4_spmd.clone, body=%wide.region_0.3_spmd.clone.sunk | while | flops 17454080 | bytes 1326441 | solution.py:115
  67.9 1.2 %all-to-all-done.2 = bf16[4,2,16384]{2,1,0:T(2,128)(2,1)S(1)} async-done(((bf16[4,2,16384]{2,1,0:T(2,128)(2,1)}), bf16[4,2,16384]{2,1,0:T(2,128)(2,1)S(1)}, u32[]{:S(2)}, u32[]{:S(2)}) %all-to-all-start.2) | async-done | bytes 262176 | tf_op jit(solution)/shard_map/all_to_all | solution.py:136
  69.9 2.3 %gather_fusion.2 = bf16[128,64,64]{2,1,0:T(8,128)(2,1)} fusion(bf16[4,12,64,64]{3,2,1,0:T(8,128)(2,1)S(1)} %pad_maximum_fusion, s32[128]{0:T(128)S(1)} %reshape.466), kind=kCustom, calls=%fused_computation.2 | custom fusion | bytes 2098176 | tf_op jit(solution)/shard_map/gather | solution.py:147
  73.3 28.2 %while.23 = (s32[]{:T(128)}, f32[2,4,4,128,64]{3,4,2,1,0:T(8,128)}, s32[2,4,16]{2,1,0:T(4,128)S(1)}, s32[2]{0:T(128)S(1)}, s32[]{:T(128)}, /*index=5*/bf16[2,4,1...) while((s32[]{:T(128)}, f32[2,4,4,128,64]{3,4,2,1,0:T(8,128)}, ...), condition=%wide.region_10.11_spmd, body=%wide.region_7.10_spmd.sunk | while | flops 562172224 | bytes 65482908 | solution.py:177
  76.2 1.4 %compare_and_fusion.5 = pred[4,128,1024]{1,2,0:T(8,128)(4,1)S(1)} fusion(s32[128]{0:T(128)S(1)} %iota_add_fusion.5, s32[4,1024]{1,0:T(4,128)S(1)} %broadcast_add_fusion.2, pred[4,1024]{1,0:T(4,128)(4,1)S(1)} %and.110), kind=kLoop, calls=%fused_computation.15.clone.1 | loop fusion | flops 1048576 | bytes 545280 | tf_op jit(solution)/shard_map/while/body/eval_jaxpr/and | solution.py:163
  77.6 2.5 %select_reduce_fusion.5 = (f32[4,4,128]{2,1,0:T(4,128)S(1)}, f32[4,4,128,16,64]{2,4,1,3,0:T(8,128)S(1)}) fusion(pred[4,128,16,64]{1,3,2,0:T(8,128)(4,1)S(1)} %compare_and_fusion.4, bf16[2,128,4,4,64]{1,4,3,2,0:T(8,128)(2,1)} %get-tuple-element.362, s32[]{:T(128)S(6)} %copy.164, bf16[2,4,16,64,64]{4,3,2,1,0:T(8,128)(2,1)} %get-tuple-element.361), kind=kOutput, calls=%fused_computation.13.clone.1 | convolution fusion | flops 274724864 | bytes 10232832 | tf_op jit(solution)/shard_map/while/body/eval_jaxpr/tghd,gnkd->ghtnk/dot_general | solution.py:154
  80.2 2.1 %select_reduce_fusion.6 = f32[4,4,128]{2,1,0:T(4,128)S(1)} fusion(f32[4,4,128,16,64]{2,4,1,3,0:T(8,128)S(1)} %get-tuple-element.322, f32[4,4,128]{2,1,0:T(4,128)S(1)} %get-tuple-element.323, pred[4,128,16,64]{1,3,2,0:T(8,128)(4,1)S(1)} %compare_and_fusion.4), kind=kLoop, calls=%fused_computation.11.clone.1 | loop fusion | flops 8386560 | bytes 8929280 | tf_op jit(solution)/shard_map/while/body/eval_jaxpr/reduce_sum | solution.py:167
  83.1 2.4 %fusion.68 = bf16[4,4,128,1024]{2,3,1,0:T(8,128)(2,1)S(1)} fusion(f32[4,4,128,16,64]{2,4,3,1,0:T(8,128)S(1)} %copy.158, f32[4,4,128]{2,1,0:T(4,128)S(1)} %get-tuple-element.323, pred[4,128,1024]{1,2,0:T(8,128)(4,1)S(1)} %compare_and_fusion.5), kind=kLoop, calls=%fused_computation.10.clone.1 | loop fusion | flops 8388608 | bytes 13115392 | tf_op jit(solution)/shard_map/while/body/eval_jaxpr/convert_element_type | solution.py:171
  90.3 1.4 %compare_and_fusion.5 = pred[4,128,1024]{1,2,0:T(8,128)(4,1)S(1)} fusion(s32[128]{0:T(128)S(1)} %iota_add_fusion.5, s32[4,1024]{1,0:T(4,128)S(1)} %broadcast_add_fusion.2, pred[4,1024]{1,0:T(4,128)(4,1)S(1)} %and.110), kind=kLoop, calls=%fused_computation.15.clone.1 | loop fusion | flops 1048576 | bytes 545280 | tf_op jit(solution)/shard_map/while/body/eval_jaxpr/and | solution.py:163
  91.8 2.5 %select_reduce_fusion.5 = (f32[4,4,128]{2,1,0:T(4,128)S(1)}, f32[4,4,128,16,64]{2,4,1,3,0:T(8,128)S(1)}) fusion(pred[4,128,16,64]{1,3,2,0:T(8,128)(4,1)S(1)} %compare_and_fusion.4, bf16[2,128,4,4,64]{1,4,3,2,0:T(8,128)(2,1)} %get-tuple-element.362, s32[]{:T(128)S(6)} %copy.164, bf16[2,4,16,64,64]{4,3,2,1,0:T(8,128)(2,1)} %get-tuple-element.361), kind=kOutput, calls=%fused_computation.13.clone.1 | convolution fusion | flops 274724864 | bytes 10232832 | tf_op jit(solution)/shard_map/while/body/eval_jaxpr/tghd,gnkd->ghtnk/dot_general | solution.py:154
  94.3 2.1 %select_reduce_fusion.6 = f32[4,4,128]{2,1,0:T(4,128)S(1)} fusion(f32[4,4,128,16,64]{2,4,1,3,0:T(8,128)S(1)} %get-tuple-element.322, f32[4,4,128]{2,1,0:T(4,128)S(1)} %get-tuple-element.323, pred[4,128,16,64]{1,3,2,0:T(8,128)(4,1)S(1)} %compare_and_fusion.4), kind=kLoop, calls=%fused_computation.11.clone.1 | loop fusion | flops 8386560 | bytes 8929280 | tf_op jit(solution)/shard_map/while/body/eval_jaxpr/reduce_sum | solution.py:167
  97.3 2.4 %fusion.68 = bf16[4,4,128,1024]{2,3,1,0:T(8,128)(2,1)S(1)} fusion(f32[4,4,128,16,64]{2,4,3,1,0:T(8,128)S(1)} %copy.158, f32[4,4,128]{2,1,0:T(4,128)S(1)} %get-tuple-element.323, pred[4,128,1024]{1,2,0:T(8,128)(4,1)S(1)} %compare_and_fusion.5), kind=kLoop, calls=%fused_computation.10.clone.1 | loop fusion | flops 8388608 | bytes 13115392 | tf_op jit(solution)/shard_map/while/body/eval_jaxpr/convert_element_type | solution.py:171
  101.5 1.5 %fusion.33 = (f32[256,4,4]{0,2,1:T(4,128)S(1)}, f32[4,4,256,64]{2,3,1,0:T(8,128)S(1)}) fusion(f32[256,4,4]{0,2,1:T(4,128)S(1)} %mul.290, f32[256,4,4]{0,2,1:T(4,128)S(1)} %mul.287, f32[4,4,256,64]{2,3,1,0:T(8,128)S(1)} %copy-done.4, f32[4,4,256]{2,1,0:T(4,128)S(1)} %broadcast_maximum_fusion.1, f32[2,4,4,128,64]{3,4,2,1,0:T(8,128)} %get-tuple-element.87), kind=kLoop, calls=%fused_computation.57 | loop fusion | flops 1568768 | bytes 3211264 | tf_op jit(solution)/shard_map/reduce_sum | solution.py:184
  103.1 2.0 %copy.107 = f32[2,128,4,4,64]{1,0,4,3,2:T(2,128)S(1)} copy(f32[2,128,4,4,64]{1,4,3,2,0:T(8,128)} %bitcast.238) | data formatting | bytes 2097152 | tf_op jit(solution)/shard_map/transpose | solution.py:180
  (165 shorter events, 38.6 us)
Async XLA Ops:
  0.0 23.6 %copy-start.5 = (bf16[1,256,1024]{2,1,0:T(8,128)(2,1)S(1)}, bf16[1,256,1024]{2,1,0:T(8,128)(2,1)}, u32[]{:S(2)}) copy-start(bf16[1,256,1024]{2,1,0:T(8,128)(2,1)} %param.12) | copy-start | bytes 1572868
  2.6 23.2 %all-to-all-start.1 = ((s32[4,4,2]{1,2,0:T(2,128)}), s32[4,4,2]{1,2,0:T(2,128)S(1)}, u32[]{:S(2)}, u32[]{:S(2)}) async-start(s32[4,4,2]{1,2,0:T(2,128)} %copy.95), calls=%async_computation.1 | async-start | bytes 8192 | tf_op jit(solution)/shard_map/all_to_all | solution.py:131
  9.6 33.9 %collective-permute-start.1 = (bf16[16,256]{1,0:T(8,128)(2,1)S(1)}, bf16[16,256]{1,0:T(8,128)(2,1)S(1)}, u32[]{:S(2)}, u32[]{:S(2)}) collective-permute-start(bf16[16,256]{1,0:T(8,128)(2,1)S(1)} %slice_bitcast_fusion.1), channel_id=1, source_target_pairs={{2,0},{4,2},{6,4},{3,1},{5,3},{7,5},{10,8},{12,10},{14,12},{11,9},... | collective-permute-start | bytes 24584 | tf_op jit(solution)/shard_map/ppermute | solution.py:21
  11.6 14.2 %collective-permute-start = (bf16[16,256]{1,0:T(8,128)(2,1)S(1)}, bf16[16,256]{1,0:T(8,128)(2,1)S(1)}, u32[]{:S(2)}, u32[]{:S(2)}) collective-permute-start(bf16[16,256]{1,0:T(8,128)(2,1)S(1)} %slice_bitcast_fusion.4), channel_id=1, source_target_pairs={{2,0},{4,2},{6,4},{3,1},{5,3},{7,5},{10,8},{12,10},{14,12},{11,9},... | collective-permute-start | bytes 24584 | tf_op jit(solution)/shard_map/ppermute | solution.py:21
  16.9 8.9 %copy-start.3 = (bf16[1,256,256]{2,1,0:T(8,128)(2,1)S(1)}, bf16[1,256,256]{2,1,0:T(8,128)(2,1)}, u32[]{:S(2)}) copy-start(bf16[1,256,256]{2,1,0:T(8,128)(2,1)} %param.13) | copy-start | bytes 393220
  23.1 20.4 %copy-start.2 = (bf16[1,256,256]{2,1,0:T(8,128)(2,1)S(1)}, bf16[1,256,256]{2,1,0:T(8,128)(2,1)}, u32[]{:S(2)}) copy-start(bf16[1,256,256]{2,1,0:T(8,128)(2,1)} %param.14) | copy-start | bytes 393220
  27.0 13.1 %all-to-all-start = ((bf16[4,2,2048]{2,1,0:T(2,128)(2,1)}), bf16[4,2,2048]{2,1,0:T(2,128)(2,1)S(1)}, u32[]{:S(2)}, u32[]{:S(2)}) async-start(bf16[4,2,2048]{2,1,0:T(2,128)(2,1)} %reshape.521), calls=%async_computation | async-start | bytes 65536 | tf_op jit(solution)/shard_map/all_to_all | solution.py:86
  40.1 18.5 %all-to-all-start.3 = ((bf16[4,2,16384]{2,1,0:T(2,128)(2,1)}), bf16[4,2,16384]{2,1,0:T(2,128)(2,1)S(1)}, u32[]{:S(2)}, u32[]{:S(2)}) async-start(bf16[4,2,16384]{2,1,0:T(2,128)(2,1)} %reshape.519), calls=%async_computation.3 | async-start | bytes 524288 | tf_op jit(solution)/shard_map/all_to_all | solution.py:137
  58.6 10.5 %all-to-all-start.2 = ((bf16[4,2,16384]{2,1,0:T(2,128)(2,1)}), bf16[4,2,16384]{2,1,0:T(2,128)(2,1)S(1)}, u32[]{:S(2)}, u32[]{:S(2)}) async-start(bf16[4,2,16384]{2,1,0:T(2,128)(2,1)} %reshape.517), calls=%async_computation.2 | async-start | bytes 524288 | tf_op jit(solution)/shard_map/all_to_all | solution.py:136
  67.5 5.7 %copy-start.6 = (s32[1,2,4,16]{3,2,1,0:T(4,128)S(1)}, s32[1,2,4,16]{3,2,1,0:T(4,128)}, u32[]{:S(2)}) copy-start(s32[1,2,4,16]{3,2,1,0:T(4,128)} %param.16) | copy-start | bytes 1540
  73.3 28.3 %copy-start.4 = (f32[4,4,256,64]{2,3,1,0:T(8,128)S(1)}, f32[4,4,256,64]{2,3,1,0:T(8,128)}, u32[]{:S(2)}) copy-start(f32[4,4,256,64]{2,3,1,0:T(8,128)} %get-tuple-element.85) | copy-start | bytes 3145732
  73.3 32.7 %copy-start.7 = (f32[1024]{0:T(1024)S(1)}, f32[1024]{0:T(1024)}, u32[]{:S(2)}) copy-start(f32[1024]{0:T(1024)} %param.19) | copy-start | bytes 12292
  83.1 2.4 %copy-start = (f32[2,4,4,128,64]{3,4,2,1,0:T(8,128)S(1)}, f32[2,4,4,128,64]{3,4,2,1,0:T(8,128)}, u32[]{:S(2)}) copy-start(f32[2,4,4,128,64]{3,4,2,1,0:T(8,128)} %get-tuple-element.347) | copy-start | bytes 3145732 | tf_op jit(solution)/shard_map/while
  86.4 1.0 copy-start.1
  97.3 2.4 %copy-start = (f32[2,4,4,128,64]{3,4,2,1,0:T(8,128)S(1)}, f32[2,4,4,128,64]{3,4,2,1,0:T(8,128)}, u32[]{:S(2)}) copy-start(f32[2,4,4,128,64]{3,4,2,1,0:T(8,128)} %get-tuple-element.347) | copy-start | bytes 3145732 | tf_op jit(solution)/shard_map/while
  100.6 1.0 copy-start.1
